TPU v7x, 32 devices: a whole 2x2x4 slice. The times are simulated.
32 devices in a mesh: sp: 4 (over z), fs: 4 (over y, x), tp: 2 (over core).
Axes of the slice: x: 2, y: 2, z: 4, core: 2. Of those that a mesh axis runs over, the one named last changes fastest.
Arguments:
- tokens: bfloat16 [4096, 2048], P('sp'), may hold values from -6 to 6
- norm_gain: float32 [2048], replicated, may hold values from 0.1 to 1.9
- w_query: bfloat16 [2048, 2048], P('sp', ('fs', 'tp')), may hold values from -3.6239223 to 3.6239223
- w_key: bfloat16 [2048, 512], P('sp', ('fs', 'tp')), may hold values from -0.088388348 to 0.088388348
- w_value: bfloat16 [2048, 512], P('sp', ('fs', 'tp')), may hold values from -0.8984375 to 0.8984375
- w_conv_in: bfloat16 [2048, 2048], P('sp', ('fs', 'tp')), may hold values from -0.125 to 0.125
- w_conv_gate: bfloat16 [2048, 2048], P('sp', ('fs', 'tp')), may hold values from -0.125 to 0.125
- conv_taps: bfloat16 [3, 2048], P(None, ('fs', 'tp')), may hold values from -3.5 to 3.5
- sink_logits: float32 [32], P(('fs', 'tp')), may hold values from 2 to 6
Outputs:
- mixed: bfloat16 [4096, 2048], P('sp', ('fs', 'tp'))
- log_sums: float32 [32, 4096], P(('fs', 'tp'), 'sp')
All inputs are finite; a program needn't handle non-finite values.
Results may differ from a plain program's by a relative error of at most 0.0077.
Values may be sent and summed in bfloat16 or wider, within the bound.
A program may use at most 64 MiB of HBM per device.

v0:
```python
import jax
import jax.numpy as jnp
from jax import lax
from jax.sharding import PartitionSpec as P

HEAD_DIM = 64
WINDOW = 128
TAPS = 3


EPS = 1e-06


def passed_along(value, axis, by):
    length = lax.axis_size(axis)
    pairs = [(i, i + by) for i in range(length) if 0 <= i + by < length]
    return lax.ppermute(value, axis, pairs)


def project_rows(normed, weights):
    return tuple(
        (jnp.dot(normed, weight, preferred_element_type=jnp.float32) for weight in weights)
    )


def block_spans(earlier_rows, current_rows, blocks, kv_local):
    joined = jnp.concatenate([earlier_rows, current_rows], axis=0).reshape(
        blocks + 1, WINDOW, kv_local, HEAD_DIM
    )
    return jnp.concatenate([joined[:-1], joined[1:]], axis=1)


def body(
    tokens, norm_gain, w_query, w_key, w_value, w_conv_in, w_conv_gate, conv_taps, sink_logits
):
    tok_rows = tokens.shape[0]
    widened = tokens.astype(jnp.float32)
    normed = (
        widened * lax.rsqrt(jnp.mean(widened * widened, axis=-1, keepdims=True) + EPS) * norm_gain
    ).astype(jnp.bfloat16)
    key_width = w_key.shape[1]
    conv_width = w_conv_in.shape[1]
    rim_rows = TAPS - 1
    weights = (w_query, w_key, w_value, w_conv_in, w_conv_gate)
    fold_weights = (
        lax.all_gather(weights[0], "sp", axis=0, tiled=True),
        lax.all_gather(weights[1], "sp", axis=0, tiled=True),
        lax.all_gather(weights[2], "sp", axis=0, tiled=True),
        lax.all_gather(weights[3], "sp", axis=0, tiled=True),
        lax.all_gather(weights[4], "sp", axis=0, tiled=True),
    )
    values = project_rows(normed, fold_weights)
    query, key_rows, value_rows, conv_in, conv_gate = tuple(
        (member.astype(jnp.bfloat16) for member in values)
    )
    outgoing = jnp.concatenate(
        [
            key_rows[tok_rows - WINDOW :].reshape(-1),
            value_rows[tok_rows - WINDOW :].reshape(-1),
            conv_in[tok_rows - rim_rows :].reshape(-1),
        ]
    )
    incoming = passed_along(outgoing, "sp", 1)
    window_size = WINDOW * key_width
    key_prev = incoming[:window_size].reshape(WINDOW, key_width)
    value_prev = incoming[window_size : 2 * window_size].reshape(WINDOW, key_width)
    conv_prev = incoming[2 * window_size :].reshape(rim_rows, conv_width)
    kv_local = key_width // HEAD_DIM
    group_size = w_query.shape[1] // key_width
    blocks = tok_rows // WINDOW
    offset = lax.axis_index("sp") * tok_rows
    query_blocks = query.reshape(blocks, WINDOW, kv_local, group_size, HEAD_DIM)
    key_span = block_spans(key_prev, key_rows, blocks, kv_local)
    value_span = block_spans(value_prev, value_rows, blocks, kv_local)
    scores = jnp.einsum(
        "nqhgd,nkhd->nhgqk", query_blocks, key_span, preferred_element_type=jnp.float32
    ) * HEAD_DIM ** (-0.5)
    block_base = offset + WINDOW * jnp.arange(blocks)[:, None, None]
    query_idx = jnp.arange(WINDOW)[None, :, None]
    key_idx = jnp.arange(2 * WINDOW)[None, None, :]
    offset_gap = query_idx + WINDOW - key_idx
    in_window = (offset_gap >= 0) & (offset_gap < WINDOW) & (block_base - WINDOW + key_idx >= 0)
    scores = jnp.where(in_window[:, None, None], scores, -jnp.inf)
    sink_col = sink_logits.reshape(kv_local, group_size)[None, :, :, None, None]
    row_top = jnp.maximum(jnp.max(scores, axis=-1, keepdims=True), sink_col)
    raised = jnp.exp(scores - row_top)
    row_sum = jnp.sum(raised, axis=-1, keepdims=True) + jnp.exp(sink_col - row_top)
    soft_weights = (raised / row_sum).astype(jnp.bfloat16)
    attended = jnp.einsum(
        "nhgqk,nkhd->nqhgd", soft_weights, value_span, preferred_element_type=jnp.float32
    ).reshape(tok_rows, kv_local * group_size * HEAD_DIM)
    log_sums = (
        (row_top + jnp.log(row_sum))[..., 0]
        .transpose(1, 2, 0, 3)
        .reshape(kv_local * group_size, tok_rows)
    )
    padded = jnp.concatenate([conv_prev, conv_in], axis=0)
    conv_sum = jnp.zeros((tok_rows, conv_width), jnp.float32)
    for tap_idx in range(TAPS):
        conv_sum = conv_sum + conv_taps[tap_idx].astype(jnp.float32) * padded[
            tap_idx : tap_idx + tok_rows
        ].astype(jnp.float32)
    convolved = conv_gate.astype(jnp.float32) * conv_sum
    mixed = (attended + convolved).astype(jnp.bfloat16)
    return (mixed, log_sums)


def solution(mesh):
    return jax.shard_map(
        body,
        mesh=mesh,
        in_specs=(
            P("sp", None),
            P(),
            P("sp", ("fs", "tp")),
            P("sp", ("fs", "tp")),
            P("sp", ("fs", "tp")),
            P("sp", ("fs", "tp")),
            P("sp", ("fs", "tp")),
            P(None, ("fs", "tp")),
            P(("fs", "tp")),
        ),
        out_specs=(P("sp", ("fs", "tp")), P(("fs", "tp"), "sp")),
        check_vma=False,
    )
```

profile of v0, /device:TPU:0, one launch (start us, length us, event | category | flops | bytes accessed | tf_op | source)
XLA Modules:
  0.0 115.6 jit_solution(15560063739411318908)
XLA Ops:
  7.2 0.7 all-gather.4.cloned.1.call-update
  8.0 0.7 all-gather.6.cloned.1.call-update
  8.7 0.7 all-gather.8.cloned.1.call-update
  9.4 3.2 %fusion = f32[1024]{0:T(1024)S(1)} fusion(bf16[1024,2048]{1,0:T(8,128)(2,1)} %param.9), kind=kLoop, calls=%fused_computation.2 | loop fusion | flops 6290432 | bytes 4198400 | tf_op jit(solution)/shard_map/reduce_sum | solution.py:39
  12.7 17.3 %all_gather.15 = bf16[2048,64]{0,1:T(8,128)(2,1)S(1)} all-gather(bf16[512,64]{0,1:T(8,128)(2,1)S(1)} %copy-done.2), channel_id=1, replica_groups=mesh['sp'=4,'fs'=4,'tp'=2] {'sp'}, dimensions={0}, use_global_device_ids=true | all-gather | bytes 327680 | tf_op jit(solution)/shard_map/all_gather | solution.py:47
  30.0 1.0 fusion.2
  31.0 1.9 %copy-done = bf16[1024,2048]{1,0:T(8,128)(2,1)} copy-done((bf16[1024,2048]{1,0:T(8,128)(2,1)}, bf16[1024,2048]{1,0:T(8,128)(2,1)S(1)}, u32[]{:S(2)}) %copy-start) | copy-done | bytes 4194328
  33.0 1.4 %convolution_convert_fusion.4 = bf16[1024,64]{0,1:T(8,128)(2,1)S(1)} fusion(bf16[1024,2048]{1,0:T(8,128)(2,1)S(1)} %fusion.2, bf16[2048,64]{0,1:T(8,128)(2,1)S(1)} %all_gather.15), kind=kOutput, calls=%fused_computation.22 | convolution fusion | flops 268500992 | bytes 4587520 | tf_op jit(solution)/shard_map/dot_general | solution.py:22
  34.4 0.1 copy.19
  34.5 0.1 reshape.209
  34.6 15.6 %all_gather.16 = bf16[2048,64]{0,1:T(8,128)(2,1)S(1)} all-gather(bf16[512,64]{0,1:T(8,128)(2,1)S(1)} %copy-done.3), channel_id=1, replica_groups=mesh['sp'=4,'fs'=4,'tp'=2] {'sp'}, dimensions={0}, use_global_device_ids=true | all-gather | bytes 327680 | tf_op jit(solution)/shard_map/all_gather | solution.py:48
  50.3 3.6 %convolution_convert_fusion.3 = bf16[1024,64]{0,1:T(8,128)(2,1)S(1)} fusion(bf16[1024,2048]{1,0:T(8,128)(2,1)} %copy-done, bf16[2048,64]{0,1:T(8,128)(2,1)S(1)} %all_gather.16), kind=kOutput, calls=%fused_computation.21 | convolution fusion | flops 268500992 | bytes 4587520 | tf_op jit(solution)/shard_map/dot_general | solution.py:22
  53.9 0.1 copy.20
  54.0 0.1 reshape.210
  54.3 0.3 broadcast_and_fusion
  54.7 4.5 %convolution_convert_fusion.2 = bf16[1024,256]{1,0:T(8,128)(2,1)} fusion(bf16[1024,2048]{1,0:T(8,128)(2,1)} %copy-done, bf16[2048,256]{1,0:T(8,128)(2,1)} %all-gather.4.cloned.1.call-done), kind=kOutput, calls=%fused_computation.20 | convolution fusion | flops 1074003968 | bytes 5767168 | tf_op jit(solution)/shard_map/dot_general | solution.py:22
  59.3 0.7 slice_bitcast_fusion
  60.0 3.4 %collective-permute-start = (bf16[16896]{0:T(1024)(128)(2,1)S(1)}, bf16[16896]{0:T(1024)(128)(2,1)S(1)}, u32[]{:S(2)}, u32[]{:S(2)}) collective-permute-start(bf16[16896]{0:T(1024)(128)(2,1)S(1)} %pad_maximum_fusion.3), channel_id=1, source_target_pairs={{0,8},{8,16},{16,24},{1,9},{9,17},{17,25},{2,10},{10,18},{18,26},{... | collective-permute-start | bytes 101384 | tf_op jit(solution)/shard_map/ppermute | solution.py:17
  63.4 10.8 %all-gather.6.cloned.1.call-done = bf16[2048,256]{1,0:T(8,128)(2,1)} async-done(((bf16[512,256]{1,0:T(8,128)(2,1)}), bf16[2048,256]{1,0:T(8,128)(2,1)}) %all-gather.6.cloned.1.call-update) | async-done | bytes 1048592 | tf_op jit(solution)/shard_map/all_gather | solution.py:46
  74.2 3.7 %convolution_convert_fusion.1 = bf16[1024,256]{1,0:T(8,128)(2,1)S(1)} fusion(bf16[1024,2048]{1,0:T(8,128)(2,1)} %copy-done, bf16[2048,256]{1,0:T(8,128)(2,1)} %all-gather.6.cloned.1.call-done), kind=kOutput, calls=%fused_computation.19 | convolution fusion | flops 1074003968 | bytes 5767168 | tf_op jit(solution)/shard_map/dot_general | solution.py:22
  77.9 0.4 reshape.225
  78.4 0.1 reshape.214
  78.4 0.1 copy.24
  78.7 0.1 copy.21
  78.9 0.9 fusion.4
  79.9 1.0 fusion.3
  81.0 1.4 %fusion.8 = f32[8,128,1,4,64]{1,4,3,0,2:T(8,128)S(1)} fusion(f32[8,4,128]{2,1,0:T(4,128)S(1)} %exponential_add_fusion, f32[8,4,128]{2,1,0:T(4,128)S(1)} %broadcast_maximum_fusion, f32[8,256,128,4]{2,1,3,0:T(8,128)S(1)} %get-tuple-element.8, pred[8,128,256]{1,2,0:T(8,128)(4,1)S(1)} %broadcast_and_fusion, bf16[8,128,1,64]{1,3,0,2:T(8,128)(2,1)S(1)} %copy.23, ...), kind=kOutput, calls=%fused_computation.13 | convolution fusion | flops 139984896 | bytes 5799936 | tf_op jit(solution)/shard_map/nhgqk,nkhd->nqhgd/dot_general | solution.py:89
  82.4 0.9 copy.38
  83.3 1.1 reshape.226
  84.4 0.7 fusion.29
  85.1 18.7 %all-gather.8.cloned.1.call-done = bf16[2048,256]{1,0:T(8,128)(2,1)} async-done(((bf16[512,256]{1,0:T(8,128)(2,1)}), bf16[2048,256]{1,0:T(8,128)(2,1)}) %all-gather.8.cloned.1.call-update) | async-done | bytes 1048592 | tf_op jit(solution)/shard_map/all_gather | solution.py:50
  103.9 5.2 %fusion.14 = bf16[1024,256]{1,0:T(8,128)(2,1)} fusion(f32[1024,256]{1,0:T(8,128)S(1)} %reshape.226, bf16[1024,2048]{1,0:T(8,128)(2,1)} %copy-done, bf16[2048,256]{1,0:T(8,128)(2,1)} %all-gather.8.cloned.1.call-done, bf16[1024,256]{1,0:T(8,128)(2,1)} %convolution_convert_fusion.2, bf16[2,256]{1,0:T(2,128)(2,1)S(1)} %slice.92, f32[256]{0:T(256)S(1)} %bitcast.102, ...), kind=kOutput, calls=%fused_computation.18 | convolution fusion | flops 1078722560 | bytes 7344128 | tf_op jit(solution)/shard_map/dot_general | solution.py:22
  (44 shorter events, 0.8 us)
Async XLA Ops:
  7.2 5.5 %copy-start.2 = (bf16[512,64]{0,1:T(8,128)(2,1)S(1)}, bf16[512,64]{0,1:T(8,128)(2,1)}, u32[]{:S(2)}) copy-start(bf16[512,64]{0,1:T(8,128)(2,1)} %param.12) | copy-start | bytes 196612
  7.2 22.8 %copy-start.4 = (f32[2048]{0:T(1024)S(1)}, f32[2048]{0:T(1024)}, u32[]{:S(2)}) copy-start(f32[2048]{0:T(1024)} %param.10) | copy-start | bytes 24580
  7.2 47.5 %all-gather.4.cloned.1.call-start = ((), (), s32[]{:S(2)}) async-start(), calls=%async_computation | async-start | bytes 1310720 | tf_op jit(solution)/shard_map/all_gather | solution.py:49
  7.9 66.3 %all-gather.6.cloned.1.call-start = ((), (), s32[]{:S(2)}) async-start(), calls=%async_computation.1 | async-start | bytes 1310720 | tf_op jit(solution)/shard_map/all_gather | solution.py:46
  8.7 95.2 %all-gather.8.cloned.1.call-start = ((), (), s32[]{:S(2)}) async-start(), calls=%async_computation.2 | async-start | bytes 1310720 | tf_op jit(solution)/shard_map/all_gather | solution.py:50
  9.4 20.6 %copy-start.1 = (bf16[1024,2048]{1,0:T(8,128)(2,1)S(1)}, bf16[1024,2048]{1,0:T(8,128)(2,1)}, u32[]{:S(2)}) copy-start(bf16[1024,2048]{1,0:T(8,128)(2,1)} %param.9) | copy-start | bytes 12582916
  31.0 2.0 %copy-start = (bf16[1024,2048]{1,0:T(8,128)(2,1)}, bf16[1024,2048]{1,0:T(8,128)(2,1)S(1)}, u32[]{:S(2)}) copy-start(bf16[1024,2048]{1,0:T(8,128)(2,1)S(1)} %fusion.2) | copy-start | bytes 12582916
  33.0 1.6 %copy-start.3 = (bf16[512,64]{0,1:T(8,128)(2,1)S(1)}, bf16[512,64]{0,1:T(8,128)(2,1)}, u32[]{:S(2)}) copy-start(bf16[512,64]{0,1:T(8,128)(2,1)} %param.13) | copy-start | bytes 196612
  34.4 19.9 %copy-start.6 = (bf16[3,256]{1,0:T(4,128)(2,1)S(1)}, bf16[3,256]{1,0:T(4,128)(2,1)}, u32[]{:S(2)}) copy-start(bf16[3,256]{1,0:T(4,128)(2,1)} %param.16) | copy-start | bytes 4612
  60.0 18.4 %collective-permute-start = (bf16[16896]{0:T(1024)(128)(2,1)S(1)}, bf16[16896]{0:T(1024)(128)(2,1)S(1)}, u32[]{:S(2)}, u32[]{:S(2)}) collective-permute-start(bf16[16896]{0:T(1024)(128)(2,1)S(1)} %pad_maximum_fusion.3), channel_id=1, source_target_pairs={{0,8},{8,16},{16,24},{1,9},{9,17},{17,25},{2,10},{10,18},{18,26},{... | collective-permute-start | bytes 101384 | tf_op jit(solution)/shard_map/ppermute | solution.py:17
  78.3 1.5 %copy-start.5 = (f32[4]{0:T(128)S(1)}, f32[4]{0:T(128)}, u32[]{:S(2)}) copy-start(f32[4]{0:T(128)} %param.17) | copy-start | bytes 52
Sparse Core Ops, SparseCore 0:
  9.6 35.5 all-gather.3
  46.7 27.3 all-gather.5
  75.8 28.0 all-gather.7
where the time goes:
time: 116 us
  blocking collectives  32.9 us (28%)
  waiting for transfers between devices  31.6 us (27%)
  matrix products  20.7 us (18%)
  between operations  14.1 us (12%)
  other arithmetic  6.64 us (6%)
  local copies, waits for them, and re-layouts  6.11 us (5%)
  starting transfers between devices  3.53 us (3%)
    all_gather x1, waiting for transfers between devices, body(): lax.all_gather(weights[4], 'sp', axis=0, tiled=True)  18.7 us
    dot_general x5, matrix products, project_rows(): jnp.dot(normed, weight, preferred_element_type=jnp.float32)  18.4 us
    all_gather x1, blocking collectives, body(): lax.all_gather(weights[1], 'sp', axis=0, tiled=True)  17.3 us
    all_gather x1, blocking collectives, body(): lax.all_gather(weights[2], 'sp', axis=0, tiled=True)  15.6 us
    all_gather x1, waiting for transfers between devices, body(): lax.all_gather(weights[0], 'sp', axis=0, tiled=True)  10.8 us
    ppermute x1, starting transfers between devices, passed_along(): return lax.ppermute(value, axis, pairs)  3.42 us
    reduce_sum x1, other arithmetic, body(): jnp.mean(widened * widened, axis=-1, keepdims=True) + EPS  3.22 us
    unnamed x20, local copies, waits for them, and re-layouts  2.75 us
  transfers between devices with their start and end apart: 4, of which 2 were waited for; matrix products, arithmetic and copies ran while one was open for 23% of the time, Pallas kernels for 0%

commit v1 on v0

v1 whole, which is shorter than its diff:
```python
import functools

import jax
import jax.numpy as jnp
from jax import lax
from jax.experimental import pallas as pl
from jax.experimental.pallas import tpu as pltpu
from jax.sharding import PartitionSpec as P

HEAD_DIM = 64
WINDOW = 128
TAPS = 3
EPS = 1e-06
LANES = 128
PAD = 8
MESH = pl.DeviceIdType.MESH


def kernel(
    n,
    tok_ref, gain_ref, wkv_ref, wq_ref, wci_ref, wcg_ref, taps_ref, sink_ref,
    mixed_ref, log_ref,
    tok, normed, kv_all, q_all, ci_all, cg_all, kv, query, attended, conv_in,
    tok_sem, own_sem, recv_sem, right_sem, left_sem, halo_send, halo_recv,
):
    me = lax.axis_index("sp")
    rows = tok.shape[0]
    depth = wq_ref.shape[0]
    shards = (wkv_ref, wq_ref, wci_ref, wcg_ref)
    wholes = (kv_all, q_all, ci_all, cg_all)
    has_left, has_right = me > 0, me < n - 1
    left, right = jnp.maximum(me - 1, 0), jnp.minimum(me + 1, n - 1)
    blocks = rows // WINDOW
    f32, bf16 = jnp.float32, jnp.bfloat16

    step_rows = rows // 4
    tok_copies = [
        pltpu.make_async_copy(
            tok_ref.at[pl.ds(i * step_rows, step_rows)], tok.at[pl.ds(i * step_rows, step_rows)], tok_sem.at[i]
        )
        for i in range(4)
    ]
    for copy in tok_copies:
        copy.start()

    def place(a, shard):
        return wholes[a].at[pl.ds(pl.multiple_of(shard * depth, depth), depth)]

    own_copies = [pltpu.make_async_copy(shards[a], place(a, me), own_sem.at[a]) for a in range(4)]
    for copy in own_copies:
        copy.start()

    barrier = pltpu.get_barrier_semaphore()

    @pl.when(has_left)
    def _():
        pl.semaphore_signal(barrier, inc=1, device_id={"sp": left}, device_id_type=MESH)

    @pl.when(has_right)
    def _():
        pl.semaphore_signal(barrier, inc=1, device_id={"sp": right}, device_id_type=MESH)

    pl.semaphore_wait(barrier, has_left.astype(jnp.int32) + has_right.astype(jnp.int32))

    def hop(a, shard, to_right, own=False):
        return pltpu.make_async_remote_copy(
            src_ref=shards[a] if own else place(a, shard),
            dst_ref=place(a, shard),
            send_sem=(right_sem if to_right else left_sem).at[a, shard],
            recv_sem=recv_sem.at[a, shard],
            device_id={"sp": right if to_right else left},
            device_id_type=MESH,
        )

    def send_own(a):
        @pl.when(has_right)
        def _():
            hop(a, me, True, True).start()

        @pl.when(has_left)
        def _():
            hop(a, me, False, True).start()

    def pass_on(a, first, last):
        def step(k, carry):
            @pl.when(me - k >= 0)
            def _():
                shard = me - k
                hop(a, shard, False).wait_recv()

                @pl.when(has_right)
                def _():
                    hop(a, shard, True).start()

            @pl.when(me + k < n)
            def _():
                shard = me + k
                hop(a, shard, True).wait_recv()

                @pl.when(has_left)
                def _():
                    hop(a, shard, False).start()

            return carry

        lax.fori_loop(first, last, step, 0)

    for a in range(3):
        send_own(a)

    norm_rows = 64
    for i in range(4):
        tok_copies[i].wait()

        @pl.loop(0, step_rows // norm_rows)
        def _(j):
            at = pl.ds(pl.multiple_of(i * step_rows + j * norm_rows, norm_rows), norm_rows)
            wide = tok[at, :].astype(f32)
            scale = lax.rsqrt(jnp.mean(wide * wide, axis=-1, keepdims=True) + EPS)
            normed[at, :] = (wide * scale * gain_ref[...]).astype(bf16)

    for copy in own_copies:
        copy.wait()

    tile = 256

    def project(a, store):
        @pl.loop(0, rows // tile)
        def _(i):
            base = pl.multiple_of(i * tile, tile)
            store(base, jnp.dot(normed[pl.ds(base, tile), :], wholes[a][...], preferred_element_type=f32))

    def halo(buffer, length, i):
        return pltpu.make_async_remote_copy(
            src_ref=buffer.at[pl.ds(rows, length)],
            dst_ref=buffer.at[pl.ds(0, length)],
            send_sem=halo_send.at[i],
            recv_sem=halo_recv.at[i],
            device_id={"sp": right},
            device_id_type=MESH,
        )

    pass_on(0, 1, n)
    send_own(3)

    def store_kv(base, value):
        kv[pl.ds(base + WINDOW, tile), :] = value.astype(bf16)

    project(0, store_kv)

    @pl.when(jnp.logical_not(has_left))
    def _():
        kv[pl.ds(0, WINDOW), :] = jnp.zeros((WINDOW, kv.shape[1]), bf16)
        conv_in[pl.ds(0, PAD), :] = jnp.zeros((PAD, conv_in.shape[1]), f32)

    pass_on(1, 1, n)

    @pl.when(has_right)
    def _():
        halo(kv, WINDOW, 0).start()

    def store_query(base, value):
        query[pl.ds(base, tile), :] = value.astype(bf16)

    project(1, store_query)

    heads = query.shape[1] // HEAD_DIM
    query_idx = lax.broadcasted_iota(jnp.int32, (WINDOW, 2 * WINDOW), 0)
    key_idx = lax.broadcasted_iota(jnp.int32, (WINDOW, 2 * WINDOW), 1)
    gap = query_idx + WINDOW - key_idx
    band = (gap >= 0) & (gap < WINDOW)
    lane = lax.broadcasted_iota(jnp.int32, (2 * WINDOW, LANES), 1)
    low = lane < HEAD_DIM
    stat_lane = lax.broadcasted_iota(jnp.int32, (WINDOW, LANES), 1)

    def attend(b, kept):
        base = pl.multiple_of(b * WINDOW, WINDOW)
        both = kv[pl.ds(base, 2 * WINDOW), :].astype(f32)
        turned = pltpu.roll(both, HEAD_DIM, 1)
        zero = jnp.zeros_like(both)
        keys = (jnp.where(low, both, zero).astype(bf16), jnp.where(low, zero, turned).astype(bf16))
        vals = (jnp.where(low, turned, zero).astype(bf16), jnp.where(low, zero, both).astype(bf16))
        stats = jnp.zeros((WINDOW, LANES), f32)
        for pair in range(heads // 2):
            cols = pl.ds(pair * LANES, LANES)
            q = query[pl.ds(base, WINDOW), cols]
            out = None
            for side in range(2):
                head = 2 * pair + side
                scores = lax.dot_general(
                    q, keys[side], (((1,), (1,)), ((), ())), preferred_element_type=f32
                ) * HEAD_DIM ** (-0.5)
                scores = jnp.where(kept, scores, -jnp.inf)
                sink = jnp.full((WINDOW, 1), sink_ref[head], f32)
                top = jnp.maximum(jnp.max(scores, axis=-1, keepdims=True), sink)
                raised = jnp.exp(scores - top)
                total = jnp.sum(raised, axis=-1, keepdims=True) + jnp.exp(sink - top)
                weights = (raised * (1.0 / total)).astype(bf16)
                part = jnp.dot(weights, vals[side], preferred_element_type=f32)
                out = part if out is None else out + part
                stats = jnp.where(stat_lane == head, top + jnp.log(total), stats)
            attended[pl.ds(base, WINDOW), cols] = out
        log_ref[:, pl.ds(base, WINDOW)] = jnp.transpose(stats)[:heads]

    def attend_range(first, last):
        @pl.loop(first, last)
        def _(b):
            attend(b, band)

    cut = [1 + (n - 1) * i // 3 for i in range(4)]
    mid = 1 + (blocks - 1) // 2
    attend_range(1, mid)
    pass_on(2, cut[0], cut[1])
    attend_range(mid, blocks)
    pass_on(2, cut[1], cut[2])

    @pl.when(has_left)
    def _():
        halo(kv, WINDOW, 0).wait_recv()

    attend(0, band & ((key_idx >= WINDOW) | has_left))
    pass_on(2, cut[2], cut[3])

    def store_conv(base, value):
        conv_in[pl.ds(base + PAD, tile), :] = value.astype(bf16).astype(f32)

    project(2, store_conv)
    pass_on(3, 1, 2)

    @pl.when(has_right)
    def _():
        halo(conv_in, PAD, 1).start()

    pass_on(3, 2, n)

    @pl.when(has_left)
    def _():
        halo(conv_in, PAD, 1).wait_recv()

    def store_mixed(base, value):
        gate = value.astype(bf16).astype(f32)
        taps = taps_ref[...].astype(f32)
        near = conv_in[pl.ds(base, tile + PAD), :]
        total = jnp.zeros_like(gate)
        for k in range(TAPS):
            start = PAD - TAPS + 1 + k
            total = total + taps[k : k + 1] * near[start : start + tile]
        mixed_ref[pl.ds(base, tile), :] = (attended[pl.ds(base, tile), :] + gate * total).astype(bf16)

    project(3, store_mixed)

    @pl.when(has_right)
    def _():
        halo(kv, WINDOW, 0).wait_send()
        halo(conv_in, PAD, 1).wait_send()

    for a in range(4):

        @pl.when(has_right)
        def _():
            @pl.loop(0, me + 1)
            def _(s):
                hop(a, s, True).wait_send()

        @pl.when(has_left)
        def _():
            @pl.loop(me, n)
            def _(s):
                hop(a, s, False).wait_send()


def body(n, tokens, norm_gain, w_query, w_key, w_value, w_conv_in, w_conv_gate, conv_taps, sink_logits):
    rows, features = tokens.shape
    width, kv_width = w_query.shape[1], w_key.shape[1] + w_value.shape[1]
    assert w_key.shape[1] == HEAD_DIM and width % LANES == 0
    w_kv = jnp.concatenate([w_key, w_value], axis=1)
    f32, bf16 = jnp.float32, jnp.bfloat16
    hbm = pl.BlockSpec(memory_space=pltpu.HBM)
    vmem = pl.BlockSpec(memory_space=pltpu.VMEM)
    smem = pl.BlockSpec(memory_space=pltpu.SMEM)
    dma = pltpu.SemaphoreType.DMA
    return pl.pallas_call(
        functools.partial(kernel, n),
        out_shape=(
            jax.ShapeDtypeStruct((rows, width), bf16),
            jax.ShapeDtypeStruct((width // HEAD_DIM, rows), f32),
        ),
        in_specs=[hbm, vmem, hbm, hbm, hbm, hbm, vmem, smem],
        out_specs=(vmem, vmem),
        scratch_shapes=[
            pltpu.VMEM((rows, features), bf16),
            pltpu.VMEM((rows, features), bf16),
            pltpu.VMEM((features, kv_width), bf16),
            pltpu.VMEM((features, width), bf16),
            pltpu.VMEM((features, width), bf16),
            pltpu.VMEM((features, width), bf16),
            pltpu.VMEM((rows + WINDOW, kv_width), bf16),
            pltpu.VMEM((rows, width), bf16),
            pltpu.VMEM((rows, width), f32),
            pltpu.VMEM((rows + PAD, width), f32),
            dma((4,)),
            dma((4,)),
            dma((4, n)),
            dma((4, n)),
            dma((4, n)),
            dma((2,)),
            dma((2,)),
        ],
        compiler_params=pltpu.CompilerParams(
            collective_id=0, has_side_effects=True, vmem_limit_bytes=60 << 20
        ),
        name="gather_attend_convolve",
    )(tokens, norm_gain.reshape(1, -1), w_kv, w_query, w_conv_in, w_conv_gate, conv_taps, sink_logits)


def solution(mesh):
    return jax.shard_map(
        functools.partial(body, mesh.shape["sp"]),
        mesh=mesh,
        in_specs=(
            P("sp", None),
            P(),
            P("sp", ("fs", "tp")),
            P("sp", ("fs", "tp")),
            P("sp", ("fs", "tp")),
            P("sp", ("fs", "tp")),
            P("sp", ("fs", "tp")),
            P(None, ("fs", "tp")),
            P(("fs", "tp")),
        ),
        out_specs=(P("sp", ("fs", "tp")), P(("fs", "tp"), "sp")),
        check_vma=False,
    )
```

time: 116 us -> 76.5 us (0.66)
  Pallas kernels: 0 us -> 69.7 us
  blocking collectives: 32.9 us -> 0 us
  waiting for transfers between devices: 31.6 us -> 0 us
  matrix products: 20.7 us -> 0 us
  between operations: 14.1 us -> 0.65 us
  other arithmetic: 6.64 us -> 0.77 us
  starting transfers between devices: 3.53 us -> 0 us
    pallas_call x0 -> x1, Pallas kernels: none -> 69.7 us  [body(): pl.pallas_call(functools.partial(kernel, n), out_shape=(jax.ShapeDtypeStr...]
    all_gather x2 -> x0, blocking collectives: 32.9 us -> none  [the longest x1 17.3 us: body(): lax.all_gather(weights[1], 'sp', axis=0, tiled=True)]
    all_gather x3 -> x0, waiting for transfers between devices: 29.6 us -> none  [the longest x1 18.7 us: body(): lax.all_gather(weights[4], 'sp', axis=0, tiled=True)]
    dot_general x7 -> x0, matrix products: 20.7 us -> none  [the longest x5 18.4 us: project_rows(): jnp.dot(normed, weight, preferred_element_type=jnp.float32)]
    reduce_sum x2 -> x0, other arithmetic: 4.25 us -> none  [the longest x1 3.22 us: body(): jnp.mean(widened * widened, axis=-1, keepdims=True) + EPS]
    ppermute x1 -> x0, starting transfers between devices: 3.42 us -> none  [passed_along(): return lax.ppermute(value, axis, pairs)]
    reshape x8 -> x0, local copies, waits for them, and re-layouts: 2.6 us -> none  [the longest x2 2.05 us: body(): attended = jnp.einsum('nhgqk,nkhd->nqhgd', soft_weights, value_span, pref...]
    unnamed x20 -> x4, local copies, waits for them, and re-layouts: 2.75 us -> 5.11 us
  transfers between devices with their start and end apart: 4 -> 0, of which waited for: 2 -> 0; matrix products, arithmetic and copies ran while one was open for 23% -> 0% of each run, Pallas kernels for 0% -> 0%
where the time goes in v1:
time: 76.5 us; the launch traced here: 76.2 us
  Pallas kernels  69.7 us (91%)
  local copies, waits for them, and re-layouts  5.11 us (7%)
  other arithmetic  0.77 us (1%)
    pallas_call x1, Pallas kernels, body(): pl.pallas_call(functools.partial(kernel, n), out_shape=(jax.ShapeDtypeStr...  69.7 us
    unnamed x4, local copies, waits for them, and re-layouts  5.11 us

profile of v1, /device:TPU:0, one launch (start us, length us, event | category | flops | bytes accessed | tf_op | source)
XLA Modules:
  0.0 76.2 jit_solution(12334521309781090709)
XLA Ops:
  0.6 1.0 %copy.11 = bf16[512,64]{1,0:T(8,128)(2,1)S(1)} copy(bf16[512,64]{0,1:T(8,128)(2,1)} %param.12) | data formatting | bytes 131072 | tf_op args[3]
  1.6 1.0 %copy.12 = bf16[512,64]{1,0:T(8,128)(2,1)S(1)} copy(bf16[512,64]{0,1:T(8,128)(2,1)} %param.13) | data formatting | bytes 131072 | tf_op args[4]
  2.6 0.8 %pad_maximum_fusion.wkv_ref = bf16[512,128]{1,0:T(8,128)(2,1)} fusion(bf16[512,64]{1,0:T(8,128)(2,1)S(1)} %copy.12, bf16[512,64]{1,0:T(8,128)(2,1)S(1)} %copy.11), kind=kLoop, calls=%fused_computation | loop fusion | flops 262144 | bytes 262144 | tf_op jit(solution)/shard_map/concatenate | solution.py:276
  3.3 69.7 %gather_attend_convolve.1 = (bf16[1024,256]{1,0:T(8,128)(2,1)}, f32[4,1024]{1,0:T(4,128)}) custom-call(bf16[1024,2048]{1,0:T(8,128)(2,1)} %tok_ref.1, f32[1,2048]{1,0:T(1,128)} %bitcast.1, bf16[512,128]{1,0:T(8,128)(2,1)} %pad_maximum_fusion.wkv_ref, bf16[512,256]{1,0:T(8,128)(2,1)} %wq_ref.1, bf16[512,256]{1,0:T(8,128)(2,1)} %wci_ref.1, ...), custom_call_target="tpu_custom_call" | custom-call | tf_op jit(solution)/shard_map/gather_attend_convolve/pallas_call | solution.py:282
  73.0 1.9 %copy.15 = bf16[1024,256]{1,0:T(8,128)(2,1)} copy(bf16[1024,256]{1,0:T(8,128)(2,1)} %get-tuple-element.4) | data formatting | bytes 1048576
  74.9 1.3 %copy.16 = f32[4,1024]{1,0:T(4,128)} copy(f32[4,1024]{1,0:T(4,128)} %get-tuple-element.5) | data formatting | bytes 32768

commit v2 on v1

--- a/solution.py
+++ b/solution.py
@@ -17,17 +17,20 @@
 
 
 def kernel(
-    n,
-    tok_ref, gain_ref, wkv_ref, wq_ref, wci_ref, wcg_ref, taps_ref, sink_ref,
-    mixed_ref, log_ref,
-    tok, normed, kv_all, q_all, ci_all, cg_all, kv, query, attended, conv_in,
-    tok_sem, own_sem, recv_sem, right_sem, left_sem, halo_send, halo_recv,
+    n, flip, tok_ref, gain_ref, *refs
 ):
+    arrays = 5 if flip else 4
+    shards = refs[:arrays]
+    (
+        taps_ref, sink_ref, mixed_ref, log_ref,
+        tok, normed, kv_all, q_all, ci_all, cg_all, kv, query, attended, conv_in, gate_sum,
+        tok_sem, own_sem, recv_sem, right_sem, left_sem, halo_send, halo_recv,
+    ) = refs[arrays:]
+    QUERY, CONV, GATE = arrays - 3, arrays - 2, arrays - 1
     me = lax.axis_index("sp")
     rows = tok.shape[0]
-    depth = wq_ref.shape[0]
-    shards = (wkv_ref, wq_ref, wci_ref, wcg_ref)
-    wholes = (kv_all, q_all, ci_all, cg_all)
+    depth = shards[QUERY].shape[0]
+    wholes = (kv_all, kv_all, q_all, ci_all, cg_all)[5 - arrays :]
     has_left, has_right = me > 0, me < n - 1
     left, right = jnp.maximum(me - 1, 0), jnp.minimum(me + 1, n - 1)
     blocks = rows // WINDOW
@@ -44,9 +47,12 @@
         copy.start()
 
     def place(a, shard):
-        return wholes[a].at[pl.ds(pl.multiple_of(shard * depth, depth), depth)]
-
-    own_copies = [pltpu.make_async_copy(shards[a], place(a, me), own_sem.at[a]) for a in range(4)]
+        at = pl.ds(pl.multiple_of(shard * depth, depth), depth)
+        if flip and a < QUERY:
+            return kv_all.at[pl.ds(a * HEAD_DIM, HEAD_DIM), at]
+        return wholes[a].at[at]
+
+    own_copies = [pltpu.make_async_copy(shards[a], place(a, me), own_sem.at[a]) for a in range(arrays)]
     for copy in own_copies:
         copy.start()
 
@@ -105,7 +111,7 @@
 
         lax.fori_loop(first, last, step, 0)
 
-    for a in range(3):
+    for a in range(GATE):
         send_own(a)
 
     norm_rows = 64
@@ -128,7 +134,16 @@
         @pl.loop(0, rows // tile)
         def _(i):
             base = pl.multiple_of(i * tile, tile)
-            store(base, jnp.dot(normed[pl.ds(base, tile), :], wholes[a][...], preferred_element_type=f32))
+            side = 1 if flip and a < QUERY else 0
+            store(
+                base,
+                lax.dot_general(
+                    normed[pl.ds(base, tile), :],
+                    wholes[a][...],
+                    (((1,), (side,)), ((), ())),
+                    preferred_element_type=f32,
+                ),
+            )
 
     def halo(buffer, length, i):
         return pltpu.make_async_remote_copy(
@@ -140,8 +155,9 @@
             device_id_type=MESH,
         )
 
-    pass_on(0, 1, n)
-    send_own(3)
+    for a in range(QUERY):
+        pass_on(a, 1, n)
+    send_own(GATE)
 
     def store_kv(base, value):
         kv[pl.ds(base + WINDOW, tile), :] = value.astype(bf16)
@@ -153,7 +169,7 @@
         kv[pl.ds(0, WINDOW), :] = jnp.zeros((WINDOW, kv.shape[1]), bf16)
         conv_in[pl.ds(0, PAD), :] = jnp.zeros((PAD, conv_in.shape[1]), f32)
 
-    pass_on(1, 1, n)
+    pass_on(QUERY, 1, n)
 
     @pl.when(has_right)
     def _():
@@ -162,7 +178,7 @@
     def store_query(base, value):
         query[pl.ds(base, tile), :] = value.astype(bf16)
 
-    project(1, store_query)
+    project(QUERY, store_query)
 
     heads = query.shape[1] // HEAD_DIM
     query_idx = lax.broadcasted_iota(jnp.int32, (WINDOW, 2 * WINDOW), 0)
@@ -210,28 +226,49 @@
     cut = [1 + (n - 1) * i // 3 for i in range(4)]
     mid = 1 + (blocks - 1) // 2
     attend_range(1, mid)
-    pass_on(2, cut[0], cut[1])
+    pass_on(CONV, cut[0], cut[1])
     attend_range(mid, blocks)
-    pass_on(2, cut[1], cut[2])
+    pass_on(CONV, cut[1], cut[2])
 
     @pl.when(has_left)
     def _():
         halo(kv, WINDOW, 0).wait_recv()
 
     attend(0, band & ((key_idx >= WINDOW) | has_left))
-    pass_on(2, cut[2], cut[3])
+    pass_on(CONV, cut[2], cut[3])
 
     def store_conv(base, value):
         conv_in[pl.ds(base + PAD, tile), :] = value.astype(bf16).astype(f32)
 
-    project(2, store_conv)
-    pass_on(3, 1, 2)
+    project(CONV, store_conv)
+    early = min(2, n - 1)
+    pass_on(GATE, 1, early)
 
     @pl.when(has_right)
     def _():
         halo(conv_in, PAD, 1).start()
 
-    pass_on(3, 2, n)
+    pass_on(GATE, early, n - 1)
+
+    far = jnp.where(2 * me >= n, 0, n - 1)
+
+    def gate_part(base, shard):
+        at = pl.ds(pl.multiple_of(shard * depth, depth), depth)
+        return jnp.dot(
+            normed[pl.ds(base, tile), at], cg_all[at, :], preferred_element_type=f32
+        )
+
+    if flip:
+
+        @pl.loop(0, rows // tile)
+        def _(i):
+            base = pl.multiple_of(i * tile, tile)
+            part = gate_part(base, lax.rem(far + 1, n))
+            for j in range(2, n):
+                part = part + gate_part(base, lax.rem(far + j, n))
+            gate_sum[pl.ds(base, tile), :] = part
+
+    pass_on(GATE, n - 1, n)
 
     @pl.when(has_left)
     def _():
@@ -247,14 +284,22 @@
             total = total + taps[k : k + 1] * near[start : start + tile]
         mixed_ref[pl.ds(base, tile), :] = (attended[pl.ds(base, tile), :] + gate * total).astype(bf16)
 
-    project(3, store_mixed)
+    if flip:
+
+        @pl.loop(0, rows // tile)
+        def _(i):
+            base = pl.multiple_of(i * tile, tile)
+            store_mixed(base, gate_sum[pl.ds(base, tile), :] + gate_part(base, far))
+
+    else:
+        project(GATE, store_mixed)
 
     @pl.when(has_right)
     def _():
         halo(kv, WINDOW, 0).wait_send()
         halo(conv_in, PAD, 1).wait_send()
 
-    for a in range(4):
+    for a in range(arrays):
 
         @pl.when(has_right)
         def _():
@@ -273,24 +318,30 @@
     rows, features = tokens.shape
     width, kv_width = w_query.shape[1], w_key.shape[1] + w_value.shape[1]
     assert w_key.shape[1] == HEAD_DIM and width % LANES == 0
-    w_kv = jnp.concatenate([w_key, w_value], axis=1)
+    depth = w_query.shape[0]
+    flip = depth % LANES == 0 and 2 < n <= 16
+    if flip:
+        w_kv, kv_shape = (w_key.T, w_value.T), (kv_width, features)
+    else:
+        w_kv, kv_shape = (jnp.concatenate([w_key, w_value], axis=1),), (features, kv_width)
+    arrays = 3 + len(w_kv)
     f32, bf16 = jnp.float32, jnp.bfloat16
     hbm = pl.BlockSpec(memory_space=pltpu.HBM)
     vmem = pl.BlockSpec(memory_space=pltpu.VMEM)
     smem = pl.BlockSpec(memory_space=pltpu.SMEM)
     dma = pltpu.SemaphoreType.DMA
     return pl.pallas_call(
-        functools.partial(kernel, n),
+        functools.partial(kernel, n, flip),
         out_shape=(
-            jax.ShapeDtypeStruct((rows, width), bf16),
-            jax.ShapeDtypeStruct((width // HEAD_DIM, rows), f32),
+            pltpu.VMEM((rows, width), bf16),
+            pltpu.VMEM((width // HEAD_DIM, rows), f32),
         ),
-        in_specs=[hbm, vmem, hbm, hbm, hbm, hbm, vmem, smem],
+        in_specs=[hbm, vmem] + [hbm] * arrays + [vmem, smem],
         out_specs=(vmem, vmem),
         scratch_shapes=[
             pltpu.VMEM((rows, features), bf16),
             pltpu.VMEM((rows, features), bf16),
-            pltpu.VMEM((features, kv_width), bf16),
+            pltpu.VMEM(kv_shape, bf16),
             pltpu.VMEM((features, width), bf16),
             pltpu.VMEM((features, width), bf16),
             pltpu.VMEM((features, width), bf16),
@@ -298,19 +349,20 @@
             pltpu.VMEM((rows, width), bf16),
             pltpu.VMEM((rows, width), f32),
             pltpu.VMEM((rows + PAD, width), f32),
+            pltpu.VMEM((rows, width), f32),
             dma((4,)),
-            dma((4,)),
-            dma((4, n)),
-            dma((4, n)),
-            dma((4, n)),
+            dma((arrays,)),
+            dma((arrays, n)),
+            dma((arrays, n)),
+            dma((arrays, n)),
             dma((2,)),
             dma((2,)),
         ],
         compiler_params=pltpu.CompilerParams(
-            collective_id=0, has_side_effects=True, vmem_limit_bytes=60 << 20
+            collective_id=0, has_side_effects=True, vmem_limit_bytes=59 << 20
         ),
         name="gather_attend_convolve",
-    )(tokens, norm_gain.reshape(1, -1), w_kv, w_query, w_conv_in, w_conv_gate, conv_taps, sink_logits)
+    )(tokens, norm_gain.reshape(1, -1), *w_kv, w_query, w_conv_in, w_conv_gate, conv_taps, sink_logits)
 
 
 def solution(mesh):

time: 76.5 us -> 70.9 us (0.927)
  local copies, waits for them, and re-layouts: 5.11 us -> 1.4 us
  Pallas kernels: 69.7 us -> 68.6 us
  other arithmetic: 0.77 us -> 0 us
    unnamed x4 -> x2, local copies, waits for them, and re-layouts: 5.11 us -> 1.4 us
    pallas_call x1, Pallas kernels: 69.7 us -> 68.6 us  [body(): pl.pallas_call(functools.partial(kernel, n, flip), out_shape=(pltpu.VMEM(...]
    concatenate x1 -> x0, other arithmetic: 0.77 us -> none  [body(): w_kv = jnp.concatenate([w_key, w_value], axis=1)]
where the time goes in v2:
time: 70.9 us; the launch traced here: 70.6 us
  Pallas kernels  68.6 us (97%)
  local copies, waits for them, and re-layouts  1.4 us (2%)
    pallas_call x1, Pallas kernels, body(): pl.pallas_call(functools.partial(kernel, n, flip), out_shape=(pltpu.VMEM(...  68.6 us

profile of v2, /device:TPU:0, one launch (start us, length us, event | category | flops | bytes accessed | tf_op | source)
XLA Modules:
  0.0 70.6 jit_solution(18116916913069561802)
XLA Ops:
  0.6 68.6 %gather_attend_convolve.1 = (bf16[1024,256]{1,0:T(8,128)(2,1)S(1)}, f32[4,1024]{1,0:T(4,128)S(1)}) custom-call(bf16[1024,2048]{1,0:T(8,128)(2,1)} %tok_ref.1, f32[1,2048]{1,0:T(1,128)} %bitcast.5, bf16[64,512]{1,0:T(8,128)(2,1)} %bitcast.3, bf16[64,512]{1,0:T(8,128)(2,1)} %bitcast.4, bf16[512,256]{1,0:T(8,128)(2,1)} %refs_2_.1, bf16[512,256]{1,0:T(8,128)(2,1)} %refs_3_.1, ...), custom_call_target="tpu_custom_call" | custom-call | tf_op jit(solution)/shard_map/gather_attend_convolve/pallas_call | solution.py:333
  69.2 0.8 %copy.13 = bf16[1024,256]{1,0:T(8,128)(2,1)} copy(bf16[1024,256]{1,0:T(8,128)(2,1)S(1)} %get-tuple-element.2) | data formatting | bytes 1048576
  70.0 0.6 copy.14

commit v3 on v2

--- a/solution.py
+++ b/solution.py
@@ -111,7 +111,7 @@
 
         lax.fori_loop(first, last, step, 0)
 
-    for a in range(GATE):
+    for a in range(arrays):
         send_own(a)
 
     norm_rows = 64
@@ -157,7 +157,6 @@
 
     for a in range(QUERY):
         pass_on(a, 1, n)
-    send_own(GATE)
 
     def store_kv(base, value):
         kv[pl.ds(base + WINDOW, tile), :] = value.astype(bf16)

time: 70.9 us -> 70.9 us (level)
  no operation moved by 1% of the time
where the time goes in v3:
time: 70.9 us; the launch traced here: 70.6 us
  Pallas kernels  68.6 us (97%)
  local copies, waits for them, and re-layouts  1.4 us (2%)
    pallas_call x1, Pallas kernels, body(): pl.pallas_call(functools.partial(kernel, n, flip), out_shape=(pltpu.VMEM(...  68.6 us

profile of v3, /device:TPU:0, one launch (start us, length us, event | category | flops | bytes accessed | tf_op | source)
XLA Modules:
  0.0 70.6 jit_solution(10250754931196991234)
XLA Ops:
  0.6 68.6 %gather_attend_convolve.1 = (bf16[1024,256]{1,0:T(8,128)(2,1)S(1)}, f32[4,1024]{1,0:T(4,128)S(1)}) custom-call(bf16[1024,2048]{1,0:T(8,128)(2,1)} %tok_ref.1, f32[1,2048]{1,0:T(1,128)} %bitcast.5, bf16[64,512]{1,0:T(8,128)(2,1)} %bitcast.3, bf16[64,512]{1,0:T(8,128)(2,1)} %bitcast.4, bf16[512,256]{1,0:T(8,128)(2,1)} %refs_2_.1, bf16[512,256]{1,0:T(8,128)(2,1)} %refs_3_.1, ...), custom_call_target="tpu_custom_call" | custom-call | tf_op jit(solution)/shard_map/gather_attend_convolve/pallas_call | solution.py:332
  69.2 0.8 %copy.13 = bf16[1024,256]{1,0:T(8,128)(2,1)} copy(bf16[1024,256]{1,0:T(8,128)(2,1)S(1)} %get-tuple-element.2) | data formatting | bytes 1048576
  70.0 0.6 copy.14
